TPU v7x, 32 devices: a whole 2x2x4 slice. The times are simulated.
32 devices in a mesh: ep: 16 (over z, x, core), tp: 2 (over y).
Axes of the slice: x: 2, y: 2, z: 4, core: 2. Of those that a mesh axis runs over, the one named last changes fastest.
Arguments:
- tokens: bfloat16 [256, 1024], P('ep'), may hold values from -6 to 6
- old_state: float32 [256, 4, 128, 128], P('ep', 'tp'), may hold values from -6 to 6
- query_weight: bfloat16 [1024, 512], P(None, 'tp'), may hold values from -0.1875 to 0.1875
- forget_weight: bfloat16 [1024, 512], P(None, 'tp'), may hold values from -0.1875 to 0.1875
- input_weight: bfloat16 [1024, 512], P(None, 'tp'), may hold values from -0.1875 to 0.1875
- lower_bound: float32 [512], P('tp'), may hold values from 0 to 0.9
- head_gain: float32 [4, 128], P('tp'), may hold values from 0.1 to 1.9
- out_weight: bfloat16 [512, 1024], P('tp'), may hold values from -0.25 to 0.25
- mix_gain: float32 [1024], replicated, may hold values from 0.1 to 1.9
- ffn_gain: float32 [1024], replicated, may hold values from 0.1 to 1.9
- group_weight: bfloat16 [1024, 4], replicated, may hold values from -0.1875 to 0.1875
- expert_weight: bfloat16 [1024, 16], replicated, may hold values from -0.1875 to 0.1875
- routes: int32 [256, 6], P('ep'), may hold values from 0 to 15, all different within a row; in each aligned block of 16 rows (0 to 15, 16 to 31, ...) at most 12 rows name the same one
- gate_weight: bfloat16 [16, 1024, 1024], P('ep', None, 'tp'), may hold values from -0.1875 to 0.1875
- up_weight: bfloat16 [16, 1024, 1024], P('ep', None, 'tp'), may hold values from -0.1875 to 0.1875
- down_weight: bfloat16 [16, 1024, 1024], P('ep', None, 'tp'), may hold values from -0.1875 to 0.1875
Outputs:
- layer_out: bfloat16 [256, 1024], P('ep', 'tp')
- new_state: float32 [256, 4, 128, 128], P('ep', 'tp')
Inputs may be any that keep to these rules, and one draw needn't show every extreme that they name: `routes`: each row names 6 different experts. In each aligned block of 16 rows (the rows of one device) no expert is named more than 12 times, a bound that some block reaches.
All inputs are finite; a program needn't handle non-finite values.
Results may differ from a plain program's by a relative error of at most 0.011.
Values may be sent and summed in bfloat16 or wider, within the bound.
A program may use at most 64 MiB of HBM per device.

v0:
```python
import jax
import jax.numpy as jnp
from jax import lax
from jax.sharding import PartitionSpec as P

epsilon = 1e-06


def scaled_rms(values, gain):
    return values * lax.rsqrt(jnp.mean(values * values, axis=-1, keepdims=True) + epsilon) * gain


def local(
    tokens,
    old_state,
    query_weight,
    forget_weight,
    input_weight,
    lower_bound,
    head_gain,
    out_weight,
    mix_gain,
    ffn_gain,
    group_weight,
    expert_weight,
    routes,
    gate_weight,
    up_weight,
    down_weight,
):
    seq_count, model_width = tokens.shape
    heads_local, head_size = (old_state.shape[1], old_state.shape[2])
    tp_size = lax.axis_size("tp")
    tp_rank = lax.axis_index("tp")
    part_width = model_width // tp_size
    resident = tokens.astype(jnp.float32)
    normed = scaled_rms(resident, mix_gain).astype(jnp.bfloat16)
    query_pre = jnp.dot(normed, query_weight, preferred_element_type=jnp.float32)
    forget_pre = jnp.dot(normed, forget_weight, preferred_element_type=jnp.float32)
    input_pre = jnp.dot(normed, input_weight, preferred_element_type=jnp.float32)
    query = jax.nn.silu(query_pre).reshape(seq_count, heads_local, head_size)
    forget = (lower_bound + (1.0 - lower_bound) * jax.nn.sigmoid(forget_pre)).reshape(
        seq_count, heads_local, head_size
    )
    value = input_pre.reshape(seq_count, heads_local, head_size)
    new_state = forget[..., None] * old_state + (1.0 - forget)[..., None] * value[:, :, None, :]
    readout = jnp.sum(new_state * query[..., None], axis=2)
    head_out = (
        scaled_rms(readout, head_gain)
        .astype(jnp.bfloat16)
        .reshape(seq_count, heads_local * head_size)
    )
    head_part = jnp.dot(head_out, out_weight, preferred_element_type=jnp.float32)
    mixed = lax.psum(head_part.astype(jnp.bfloat16), "tp")
    residual = (resident + mixed.astype(jnp.float32)).astype(jnp.bfloat16)
    ffn_in = scaled_rms(residual.astype(jnp.float32), ffn_gain).astype(jnp.bfloat16)
    experts = expert_weight.shape[1]
    groups = group_weight.shape[1]
    top_count = routes.shape[1]
    group_raw = jnp.exp(jnp.dot(ffn_in, group_weight, preferred_element_type=jnp.float32))
    group_prob = group_raw / jnp.sum(group_raw, axis=-1, keepdims=True)
    expert_raw = jnp.exp(
        jnp.dot(ffn_in, expert_weight, preferred_element_type=jnp.float32)
    ).reshape(seq_count, groups, experts // groups)
    expert_prob = (
        expert_raw / jnp.sum(expert_raw, axis=-1, keepdims=True) * group_prob[:, :, None]
    ).reshape(seq_count, experts)
    expert_ids = jnp.arange(experts, dtype=jnp.int32)
    chosen = routes[:, :, None] == expert_ids[None, None, :]
    weight = jnp.sum(jnp.where(chosen, expert_prob[:, None, :], 0.0), axis=-1)
    gate = weight / jnp.sum(weight, axis=-1, keepdims=True)
    capacity = min(seq_count, max(2, 2 * seq_count * top_count // experts))
    flat = routes.reshape(-1)
    hits = (flat[:, None] == expert_ids[None, :]).astype(jnp.int32)
    before = jnp.cumsum(hits, axis=0) - hits
    slots = jnp.sum(hits * before, axis=1)
    target = flat * capacity + slots
    slot_ids = jnp.arange(experts * capacity, dtype=jnp.int32)
    spread = jnp.sum(
        (slot_ids[:, None, None] == target.reshape(seq_count, top_count)[None, :, :]).astype(
            jnp.int32
        ),
        axis=2,
    ).astype(jnp.bfloat16)
    choose = (target[:, None] == slot_ids[None, :]).astype(jnp.bfloat16)
    outgoing = (
        jnp.dot(spread, ffn_in, preferred_element_type=jnp.float32)
        .astype(jnp.bfloat16)
        .reshape(experts, capacity, model_width)
    )
    arrived = lax.all_to_all(outgoing, "ep", split_axis=0, concat_axis=1, tiled=True)
    gate_hidden = jnp.einsum(
        "erd,edf->erf", arrived, gate_weight, preferred_element_type=jnp.float32
    )
    up_hidden = jnp.einsum("erd,edf->erf", arrived, up_weight, preferred_element_type=jnp.float32)
    hidden = (jax.nn.silu(gate_hidden) * up_hidden).astype(jnp.bfloat16)
    produced = jnp.einsum(
        "erf,efd->erd",
        lax.all_gather(hidden, "tp", axis=2, tiled=True),
        down_weight,
        preferred_element_type=jnp.float32,
    ).astype(jnp.bfloat16)
    returned = lax.all_to_all(produced, "ep", split_axis=1, concat_axis=0, tiled=True)
    picked = jnp.dot(
        choose, returned.reshape(experts * capacity, part_width), preferred_element_type=jnp.float32
    ).reshape(seq_count, top_count, part_width)
    mixture = jnp.sum(gate[:, :, None] * picked, axis=1)
    own_resid = lax.dynamic_slice_in_dim(residual, tp_rank * part_width, part_width, 1).astype(
        jnp.float32
    )
    layer_out = (own_resid + mixture).astype(jnp.bfloat16)
    return (layer_out, new_state)


def solution(mesh):
    in_specs = (
        P("ep", None),
        P("ep", "tp", None, None),
        P(None, "tp"),
        P(None, "tp"),
        P(None, "tp"),
        P("tp"),
        P("tp", None),
        P("tp", None),
        P(),
        P(),
        P(),
        P(),
        P("ep", None),
        P("ep", None, "tp"),
        P("ep", None, "tp"),
        P("ep", None, "tp"),
    )
    out_specs = (P("ep", "tp"), P("ep", "tp", None, None))
    return jax.shard_map(local, mesh=mesh, in_specs=in_specs, out_specs=out_specs, check_vma=False)
```

profile of v0, /device:TPU:0, one launch (start us, length us, event | category | flops | bytes accessed | tf_op | source)
XLA Modules:
  0.0 71.4 jit_solution(7429910828382578727)
XLA Ops:
  0.6 0.0 copy-start
  0.7 0.9 %copy.77 = s32[16,6]{1,0:T(8,128)S(1)} copy(s32[16,6]{0,1:T(8,128)} %param.28) | data formatting | bytes 768 | tf_op args[12]
  1.6 0.1 eq.73
  1.7 0.1 fusion.25
  1.8 0.1 reduce_window_sum.11
  1.9 0.2 select_reduce_fusion.2
  2.1 0.1 reduce_sum.110
  2.1 0.1 copy.78
  2.2 0.7 multiply_add_fusion.1
  2.9 0.1 convert_reduce_fusion
  3.0 0.9 %fusion.20 = f32[16]{0:T(128)S(1)} fusion(bf16[16,1024]{1,0:T(8,128)(2,1)} %param.16), kind=kLoop, calls=%fused_computation.37 | loop fusion | flops 49136 | bytes 32832 | tf_op jit(solution)/shard_map/reduce_sum | solution.py:10
  3.9 1.3 %divide_multiply_fusion = f32[16,256]{1,0:T(8,128)S(1)} fusion(bf16[1024,256]{1,0:T(8,128)(2,1)} %param.18, bf16[16,1024]{1,0:T(8,128)(2,1)} %param.16, f32[1024]{0:T(1024)} %param.24, f32[16]{0:T(128)S(1)} %add_rsqrt_fusion.2), kind=kOutput, calls=%fused_computation.53 | convolution fusion | flops 8470528 | bytes 577600 | tf_op jit(solution)/shard_map/dot_general | solution.py:38
  5.3 1.3 %fusion.33 = f32[16,256]{1,0:T(8,128)S(1)} fusion(bf16[1024,256]{1,0:T(8,128)(2,1)} %param.20, bf16[16,1024]{1,0:T(8,128)(2,1)} %param.16, f32[1024]{0:T(1024)} %param.24, f32[16]{0:T(128)S(1)} %add_rsqrt_fusion.2), kind=kOutput, calls=%fused_computation.67 | convolution fusion | flops 8454144 | bytes 577600 | tf_op jit(solution)/shard_map/dot_general | solution.py:40
  6.6 0.7 broadcast_subtract_fusion.1
  7.3 1.3 %fusion.8 = f32[16,256]{1,0:T(8,128)S(1)} fusion(bf16[1024,256]{1,0:T(8,128)(2,1)} %param.19, f32[256]{0:T(256)S(1)} %broadcast_subtract_fusion.1, f32[256]{0:T(256)} %param.21, bf16[16,1024]{1,0:T(8,128)(2,1)} %param.16, f32[1024]{0:T(1024)} %param.24, f32[16]{0:T(128)S(1)} %add_rsqrt_fusion.2), kind=kOutput, calls=%fused_computation.16 | convolution fusion | flops 8474624 | bytes 579648 | tf_op jit(solution)/shard_map/dot_general | solution.py:39
  8.6 0.0 copy-start.3
  8.7 0.0 copy-start.5
  8.7 3.0 %multiply_reduce_fusion = (f32[16,2,128]{2,1,0:T(2,128)S(1)}, f32[16,2,128,128]{3,2,1,0:T(8,128)}) fusion(f32[16,2,128]{2,1,0:T(2,128)S(1)} %mul.173, f32[16,2,128]{2,1,0:T(2,128)S(1)} %mul.169, f32[16,2,128]{2,1,0:T(2,128)S(1)} %broadcast_subtract_fusion, f32[16,2,128,128]{3,2,1,0:T(8,128)S(1)} %copy-done.1, f32[16,2,128]{2,1,0:T(2,128)S(1)} %mul.165), kind=kLoop, calls=%fused_computation.1 | loop fusion | flops 2617344 | bytes 4276224 | tf_op jit(solution)/shard_map/reduce_sum | solution.py:47
  11.7 0.1 fusion.27
  11.8 0.1 copy.73
  11.9 0.1 broadcast_multiply_fusion
  12.0 1.2 %convolution_convert_fusion.2 = bf16[16,1024]{1,0:T(8,128)(2,1)S(1)} fusion(bf16[256,1024]{1,0:T(8,128)(2,1)} %param.23, f32[2,8,2,128]{3,2,1,0:T(2,128)S(1)} %bitcast.43, f32[256]{0:T(256)S(1)} %bitcast.47), kind=kOutput, calls=%fused_computation.10 | convolution fusion | flops 8413184 | bytes 574464 | tf_op jit(solution)/shard_map/dot_general | solution.py:53
  13.2 10.0 %psum.7 = bf16[16,1024]{1,0:T(8,128)(2,1)S(1)} all-reduce(bf16[16,1024]{1,0:T(8,128)(2,1)S(1)} %convolution_convert_fusion.2), channel_id=1, replica_groups=mesh['ep'=16,'tp'=2] {'tp'}, use_global_device_ids=true, to_apply=%region_3.4 | all-reduce | flops 16384 | bytes 65536 | tf_op jit(solution)/shard_map/psum | solution.py:54
  23.2 0.1 fusion.17
  23.3 0.3 convolution_convert_fusion
  23.6 0.9 %reshape.168 = bf16[16,12,1024]{2,1,0:T(8,128)(2,1)} reshape(bf16[192,1024]{1,0:T(8,128)(2,1)S(1)} %convolution_convert_fusion) | data formatting | bytes 786432 | tf_op jit(solution)/shard_map/reshape | solution.py:89
  24.5 5.9 %all-to-all-start = ((bf16[16,12,1024]{2,1,0:T(8,128)(2,1)}), bf16[16,12,1024]{2,1,0:T(8,128)(2,1)S(1)}, u32[]{:S(2)}, u32[]{:S(2)}) async-start(bf16[16,12,1024]{2,1,0:T(8,128)(2,1)} %reshape.168), calls=%async_computation | async-start | bytes 1048576 | tf_op jit(solution)/shard_map/all_to_all | solution.py:91
  30.5 0.2 fusion.42
  30.7 0.1 copy.76
  30.8 0.2 convolution_exponential_fusion
  31.0 0.1 copy.74
  31.1 0.1 copy.75
  31.1 13.6 %all-to-all-done = bf16[16,12,1024]{2,1,0:T(8,128)(2,1)S(1)} async-done(((bf16[16,12,1024]{2,1,0:T(8,128)(2,1)}), bf16[16,12,1024]{2,1,0:T(8,128)(2,1)S(1)}, u32[]{:S(2)}, u32[]{:S(2)}) %all-to-all-start) | async-done | bytes 393248 | tf_op jit(solution)/shard_map/all_to_all | solution.py:91
  44.7 0.1 reshape.169
  44.8 0.4 fusion.11
  45.2 0.4 fusion.1
  45.6 7.6 %all-gather = bf16[192,1024]{1,0:T(8,128)(2,1)S(1)} all-gather(bf16[192,512]{1,0:T(8,128)(2,1)S(1)} %fusion.1), channel_id=2, replica_groups=mesh['ep'=16,'tp'=2] {'tp'}, dimensions={1}, use_global_device_ids=true | all-gather | bytes 589824 | tf_op jit(solution)/shard_map/all_gather | solution.py:99
  53.2 0.4 fusion.2
  53.6 0.3 copy.92
  53.9 0.5 broadcast.119
  54.4 1.8 %reduce.1 = bf16[192,512]{1,0:T(8,128)(2,1)S(1)} reduce(bf16[192,1,512]{2,1,0:T(2,128)(2,1)S(1)} %bitcast.41, bf16[]{:T(256)} %broadcast.119), dimensions={1}, to_apply=%bitcast.40.reduce_sub_computation | reduce | bytes 393218
  56.3 0.8 %reshape.179 = bf16[16,2,3072]{2,1,0:T(2,128)(2,1)} reshape(bf16[192,512]{1,0:T(8,128)(2,1)S(1)} %reduce.1) | data formatting | bytes 393216
  57.0 4.4 %all-to-all-start.1 = ((bf16[16,2,3072]{2,1,0:T(2,128)(2,1)}), bf16[16,2,3072]{2,1,0:T(2,128)(2,1)S(1)}, u32[]{:S(2)}, u32[]{:S(2)}) async-start(bf16[16,2,3072]{2,1,0:T(2,128)(2,1)} %reshape.179), calls=%async_computation.1 | async-start | bytes 393216 | tf_op jit(solution)/shard_map/all_to_all | solution.py:103
  61.5 0.2 select_reduce_fusion
  61.7 8.7 %all-to-all-done.1 = bf16[16,2,3072]{2,1,0:T(2,128)(2,1)S(1)} async-done(((bf16[16,2,3072]{2,1,0:T(2,128)(2,1)}), bf16[16,2,3072]{2,1,0:T(2,128)(2,1)S(1)}, u32[]{:S(2)}, u32[]{:S(2)}) %all-to-all-start.1) | async-done | bytes 196640 | tf_op jit(solution)/shard_map/all_to_all | solution.py:103
  70.4 0.1 reshape.180
  70.5 0.2 fusion.3
  70.8 0.6 add_convert_fusion
  (29 shorter events, 0.2 us)
Async XLA Ops:
  0.6 44.2 %copy-start = (bf16[1,1024,512]{2,1,0:T(8,128)(2,1)S(1)}, bf16[1,1024,512]{2,1,0:T(8,128)(2,1)}, u32[]{:S(2)}) copy-start(bf16[1,1024,512]{2,1,0:T(8,128)(2,1)} %param.29) | copy-start | bytes 3145732
  0.6 8.0 %copy-start.1 = (f32[16,2,128,128]{3,2,1,0:T(8,128)S(1)}, f32[16,2,128,128]{3,2,1,0:T(8,128)}, u32[]{:S(2)}) copy-start(f32[16,2,128,128]{3,2,1,0:T(8,128)} %param.17) | copy-start | bytes 6291460
  8.6 3.4 %copy-start.6 = (f32[2,128]{1,0:T(2,128)S(1)}, f32[2,128]{1,0:T(2,128)}, u32[]{:S(2)}) copy-start(f32[2,128]{1,0:T(2,128)} %param.22) | copy-start | bytes 3076
  8.6 14.5 %copy-start.3 = (bf16[16,1024]{1,0:T(8,128)(2,1)S(1)}, bf16[16,1024]{1,0:T(8,128)(2,1)}, u32[]{:S(2)}) copy-start(bf16[16,1024]{1,0:T(8,128)(2,1)} %param.16) | copy-start | bytes 98308
  8.7 14.7 %copy-start.5 = (f32[1024]{0:T(1024)S(1)}, f32[1024]{0:T(1024)}, u32[]{:S(2)}) copy-start(f32[1024]{0:T(1024)} %param.25) | copy-start | bytes 12292
  11.7 18.8 %copy-start.9 = (bf16[1024,4]{0,1:T(4,128)(2,1)S(1)}, bf16[1024,4]{0,1:T(4,128)(2,1)}, u32[]{:S(2)}) copy-start(bf16[1024,4]{0,1:T(4,128)(2,1)} %param.26) | copy-start | bytes 24580
  11.7 19.1 %copy-start.8 = (bf16[1024,16]{0,1:T(8,128)(2,1)S(1)}, bf16[1024,16]{0,1:T(8,128)(2,1)}, u32[]{:S(2)}) copy-start(bf16[1024,16]{0,1:T(8,128)(2,1)} %param.27) | copy-start | bytes 98308
  24.5 20.7 %copy-start.7 = (bf16[1,1024,512]{2,1,0:T(8,128)(2,1)S(1)}, bf16[1,1024,512]{2,1,0:T(8,128)(2,1)}, u32[]{:S(2)}) copy-start(bf16[1,1024,512]{2,1,0:T(8,128)(2,1)} %param.30) | copy-start | bytes 3145732
  24.5 20.2 %all-to-all-start = ((bf16[16,12,1024]{2,1,0:T(8,128)(2,1)}), bf16[16,12,1024]{2,1,0:T(8,128)(2,1)S(1)}, u32[]{:S(2)}, u32[]{:S(2)}) async-start(bf16[16,12,1024]{2,1,0:T(8,128)(2,1)} %reshape.168), calls=%async_computation | async-start | bytes 1048576 | tf_op jit(solution)/shard_map/all_to_all | solution.py:91
  45.2 8.0 %copy-start.2 = (bf16[1,1024,512]{2,1,0:T(8,128)(2,1)S(1)}, bf16[1,1024,512]{2,1,0:T(8,128)(2,1)}, u32[]{:S(2)}) copy-start(bf16[1,1024,512]{2,1,0:T(8,128)(2,1)} %param.31) | copy-start | bytes 3145732
  45.6 15.8 %copy-start.4 = (s32[16,6]{0,1:T(8,128)S(1)}, s32[16,6]{0,1:T(8,128)}, u32[]{:S(2)}) copy-start(s32[16,6]{0,1:T(8,128)} %param.28) | copy-start | bytes 1156
  57.0 13.4 %all-to-all-start.1 = ((bf16[16,2,3072]{2,1,0:T(2,128)(2,1)}), bf16[16,2,3072]{2,1,0:T(2,128)(2,1)S(1)}, u32[]{:S(2)}, u32[]{:S(2)}) async-start(bf16[16,2,3072]{2,1,0:T(2,128)(2,1)} %reshape.179), calls=%async_computation.1 | async-start | bytes 393216 | tf_op jit(solution)/shard_map/all_to_all | solution.py:103
where the time goes:
time: 71.9 us; the launch traced here: 71.4 us
  waiting for transfers between devices  22.3 us (31%)
  blocking collectives  17.6 us (24%)
  starting transfers between devices  10.3 us (14%)
  other arithmetic  8.77 us (12%)
  matrix products  7.21 us (10%)
  local copies, waits for them, and re-layouts  4.28 us (6%)
  between operations  0.95 us (1%)
    all_to_all x1, waiting for transfers between devices, local(): lax.all_to_all(outgoing, 'ep', split_axis=0, concat_axis=1, tiled=True)  13.6 us
    psum x1, blocking collectives, local(): mixed = lax.psum(head_part.astype(jnp.bfloat16), 'tp')  9.95 us
    all_to_all x1, waiting for transfers between devices, local(): lax.all_to_all(produced, 'ep', split_axis=1, concat_axis=0, tiled=True)  8.72 us
    all_gather x1, blocking collectives, local(): lax.all_gather(hidden, 'tp', axis=2, tiled=True)  7.6 us
    all_to_all x1, starting transfers between devices, local(): lax.all_to_all(outgoing, 'ep', split_axis=0, concat_axis=1, tiled=True)  5.92 us
    all_to_all x1, starting transfers between devices, local(): lax.all_to_all(produced, 'ep', split_axis=1, concat_axis=0, tiled=True)  4.41 us
    reduce_sum x1, other arithmetic, local(): readout = jnp.sum(new_state * query[..., None], axis=2)  3.02 us
    unnamed x24, local copies, waits for them, and re-layouts  2.4 us
  transfers between devices with their start and end apart: 2, of which 2 were waited for; matrix products, arithmetic and copies ran while one was open for 1% of the time, Pallas kernels for 0%

commit v1 on v0

--- a/solution.py
+++ b/solution.py
@@ -51,7 +51,7 @@
         .reshape(seq_count, heads_local * head_size)
     )
     head_part = jnp.dot(head_out, out_weight, preferred_element_type=jnp.float32)
-    mixed = lax.psum(head_part.astype(jnp.bfloat16), "tp")
+    mixed = jnp.sum(lax.all_gather(head_part.astype(jnp.bfloat16), "tp"), axis=0)
     residual = (resident + mixed.astype(jnp.float32)).astype(jnp.bfloat16)
     ffn_in = scaled_rms(residual.astype(jnp.float32), ffn_gain).astype(jnp.bfloat16)
     experts = expert_weight.shape[1]

time: 71.9 us -> 68.2 us (0.949)
  blocking collectives: 17.6 us -> 13.2 us
    psum x1 -> x0, blocking collectives: 9.95 us -> none  [local(): mixed = lax.psum(head_part.astype(jnp.bfloat16), 'tp')]
    all_gather x0 -> x1, blocking collectives: none -> 5.53 us  [local(): lax.all_gather(head_part.astype(jnp.bfloat16), 'tp')]
where the time goes in v1:
time: 68.2 us; the launch traced here: 67.6 us
  waiting for transfers between devices  22.3 us (33%)
  blocking collectives  13.2 us (19%)
  starting transfers between devices  11 us (16%)
  other arithmetic  8.78 us (13%)
  matrix products  7.19 us (11%)
  local copies, waits for them, and re-layouts  4.28 us (6%)
  between operations  0.95 us (1%)
    all_to_all x1, waiting for transfers between devices, local(): lax.all_to_all(outgoing, 'ep', split_axis=0, concat_axis=1, tiled=True)  13.6 us
    all_to_all x1, waiting for transfers between devices, local(): lax.all_to_all(produced, 'ep', split_axis=1, concat_axis=0, tiled=True)  8.72 us
    all_gather x1, blocking collectives, local(): lax.all_gather(hidden, 'tp', axis=2, tiled=True)  7.62 us
    all_to_all x1, starting transfers between devices, local(): lax.all_to_all(outgoing, 'ep', split_axis=0, concat_axis=1, tiled=True)  6.57 us
    all_gather x1, blocking collectives, local(): lax.all_gather(head_part.astype(jnp.bfloat16), 'tp')  5.53 us
    all_to_all x1, starting transfers between devices, local(): lax.all_to_all(produced, 'ep', split_axis=1, concat_axis=0, tiled=True)  4.41 us
    reduce_sum x1, other arithmetic, local(): readout = jnp.sum(new_state * query[..., None], axis=2)  3.02 us
    unnamed x24, local copies, waits for them, and re-layouts  2.4 us
  transfers between devices with their start and end apart: 2, of which 2 were waited for; matrix products, arithmetic and copies ran while one was open for 1% of the time, Pallas kernels for 0%

profile of v1, /device:TPU:0, one launch (start us, length us, event | category | flops | bytes accessed | tf_op | source)
XLA Modules:
  0.0 67.6 jit_solution(4205302458017341384)
XLA Ops:
  0.6 0.0 copy-start
  0.7 0.9 %copy.77 = s32[16,6]{1,0:T(8,128)S(1)} copy(s32[16,6]{0,1:T(8,128)} %param.28) | data formatting | bytes 768 | tf_op args[12]
  1.6 0.1 eq.73
  1.7 0.1 fusion.25
  1.8 0.1 reduce_window_sum.11
  1.9 0.2 select_reduce_fusion.2
  2.1 0.1 reduce_sum.123
  2.1 0.1 copy.78
  2.2 0.7 %multiply_add_fusion.1 = s32[16,6]{0,1:T(8,128)S(1)} fusion(s32[16,6]{0,1:T(8,128)S(1)} %copy.78, s32[16,6]{0,1:T(8,128)} %param.28), kind=kLoop, calls=%fused_computation.59 | loop fusion | flops 192 | bytes 1152 | tf_op jit(solution)/shard_map/add | solution.py:77
  2.9 0.1 convert_reduce_fusion
  3.0 0.9 %fusion.20 = f32[16]{0:T(128)S(1)} fusion(bf16[16,1024]{1,0:T(8,128)(2,1)} %param.16), kind=kLoop, calls=%fused_computation.37 | loop fusion | flops 49136 | bytes 32832 | tf_op jit(solution)/shard_map/reduce_sum | solution.py:10
  3.9 1.3 %divide_multiply_fusion = f32[16,256]{1,0:T(8,128)S(1)} fusion(bf16[1024,256]{1,0:T(8,128)(2,1)} %param.18, bf16[16,1024]{1,0:T(8,128)(2,1)} %param.16, f32[1024]{0:T(1024)} %param.24, f32[16]{0:T(128)S(1)} %add_rsqrt_fusion.2), kind=kOutput, calls=%fused_computation.53 | convolution fusion | flops 8470528 | bytes 577600 | tf_op jit(solution)/shard_map/dot_general | solution.py:38
  5.3 1.3 %fusion.33 = f32[16,256]{1,0:T(8,128)S(1)} fusion(bf16[1024,256]{1,0:T(8,128)(2,1)} %param.20, bf16[16,1024]{1,0:T(8,128)(2,1)} %param.16, f32[1024]{0:T(1024)} %param.24, f32[16]{0:T(128)S(1)} %add_rsqrt_fusion.2), kind=kOutput, calls=%fused_computation.67 | convolution fusion | flops 8454144 | bytes 577600 | tf_op jit(solution)/shard_map/dot_general | solution.py:40
  6.6 0.7 %broadcast_subtract_fusion.1 = f32[256]{0:T(256)S(1)} fusion(f32[256]{0:T(256)} %param.21), kind=kLoop, calls=%fused_computation.65 | loop fusion | flops 256 | bytes 2048 | tf_op jit(solution)/shard_map/sub | solution.py:42
  7.3 1.3 %fusion.8 = f32[16,256]{1,0:T(8,128)S(1)} fusion(bf16[1024,256]{1,0:T(8,128)(2,1)} %param.19, f32[256]{0:T(256)S(1)} %broadcast_subtract_fusion.1, f32[256]{0:T(256)} %param.21, bf16[16,1024]{1,0:T(8,128)(2,1)} %param.16, f32[1024]{0:T(1024)} %param.24, f32[16]{0:T(128)S(1)} %add_rsqrt_fusion.2), kind=kOutput, calls=%fused_computation.16 | convolution fusion | flops 8474624 | bytes 579648 | tf_op jit(solution)/shard_map/dot_general | solution.py:39
  8.6 0.0 copy-start.3
  8.7 0.0 copy-start.5
  8.7 3.0 %multiply_reduce_fusion = (f32[16,2,128]{2,1,0:T(2,128)S(1)}, f32[16,2,128,128]{3,2,1,0:T(8,128)}) fusion(f32[16,2,128]{2,1,0:T(2,128)S(1)} %mul.173, f32[16,2,128]{2,1,0:T(2,128)S(1)} %mul.169, f32[16,2,128]{2,1,0:T(2,128)S(1)} %broadcast_subtract_fusion, f32[16,2,128,128]{3,2,1,0:T(8,128)S(1)} %copy-done.1, f32[16,2,128]{2,1,0:T(2,128)S(1)} %mul.165), kind=kLoop, calls=%fused_computation.1 | loop fusion | flops 2617344 | bytes 4276224 | tf_op jit(solution)/shard_map/reduce_sum | solution.py:47
  11.7 0.1 fusion.27
  11.8 0.1 copy.73
  11.9 0.1 broadcast_multiply_fusion
  12.0 1.2 %convolution_convert_fusion.2 = bf16[16,1024]{1,0:T(8,128)(2,1)S(1)} fusion(bf16[256,1024]{1,0:T(8,128)(2,1)} %param.23, f32[2,8,2,128]{3,2,1,0:T(2,128)S(1)} %bitcast.45, f32[256]{0:T(256)S(1)} %bitcast.49), kind=kOutput, calls=%fused_computation.10 | convolution fusion | flops 8413184 | bytes 574464 | tf_op jit(solution)/shard_map/dot_general | solution.py:53
  13.2 5.5 %all-gather = bf16[32,1024]{1,0:T(8,128)(2,1)S(1)} all-gather(bf16[16,1024]{1,0:T(8,128)(2,1)S(1)} %convolution_convert_fusion.2), channel_id=2, replica_groups=mesh['ep'=16,'tp'=2] {'tp'}, dimensions={0}, use_global_device_ids=true | all-gather | bytes 98304 | tf_op jit(solution)/shard_map/all_gather | solution.py:54
  18.8 0.1 fusion.17
  18.9 0.3 convolution_convert_fusion
  19.2 0.9 %reshape.168 = bf16[16,12,1024]{2,1,0:T(8,128)(2,1)} reshape(bf16[192,1024]{1,0:T(8,128)(2,1)S(1)} %convolution_convert_fusion) | data formatting | bytes 786432 | tf_op jit(solution)/shard_map/reshape | solution.py:89
  20.1 6.6 %all-to-all-start = ((bf16[16,12,1024]{2,1,0:T(8,128)(2,1)}), bf16[16,12,1024]{2,1,0:T(8,128)(2,1)S(1)}, u32[]{:S(2)}, u32[]{:S(2)}) async-start(bf16[16,12,1024]{2,1,0:T(8,128)(2,1)} %reshape.168), calls=%async_computation | async-start | bytes 1048576 | tf_op jit(solution)/shard_map/all_to_all | solution.py:91
  26.7 0.2 fusion.42
  26.9 0.1 copy.76
  27.0 0.2 convolution_exponential_fusion
  27.2 0.1 copy.74
  27.3 0.1 copy.75
  27.4 13.6 %all-to-all-done = bf16[16,12,1024]{2,1,0:T(8,128)(2,1)S(1)} async-done(((bf16[16,12,1024]{2,1,0:T(8,128)(2,1)}), bf16[16,12,1024]{2,1,0:T(8,128)(2,1)S(1)}, u32[]{:S(2)}, u32[]{:S(2)}) %all-to-all-start) | async-done | bytes 393248 | tf_op jit(solution)/shard_map/all_to_all | solution.py:91
  41.0 0.1 reshape.169
  41.1 0.4 fusion.11
  41.5 0.4 fusion.1
  41.8 7.6 %all-gather.1 = bf16[192,1024]{1,0:T(8,128)(2,1)S(1)} all-gather(bf16[192,512]{1,0:T(8,128)(2,1)S(1)} %fusion.1), channel_id=3, replica_groups=mesh['ep'=16,'tp'=2] {'tp'}, dimensions={1}, use_global_device_ids=true | all-gather | bytes 589824 | tf_op jit(solution)/shard_map/all_gather | solution.py:99
  49.5 0.4 fusion.2
  49.9 0.3 copy.92
  50.2 0.5 broadcast.119
  50.7 1.8 %reduce.2 = bf16[192,512]{1,0:T(8,128)(2,1)S(1)} reduce(bf16[192,1,512]{2,1,0:T(2,128)(2,1)S(1)} %bitcast.42, bf16[]{:T(256)} %broadcast.119), dimensions={1}, to_apply=%bitcast.41.reduce_sub_computation | reduce | bytes 393218
  52.5 0.8 %reshape.180 = bf16[16,2,3072]{2,1,0:T(2,128)(2,1)} reshape(bf16[192,512]{1,0:T(8,128)(2,1)S(1)} %reduce.2) | data formatting | bytes 393216
  53.3 4.4 %all-to-all-start.1 = ((bf16[16,2,3072]{2,1,0:T(2,128)(2,1)}), bf16[16,2,3072]{2,1,0:T(2,128)(2,1)S(1)}, u32[]{:S(2)}, u32[]{:S(2)}) async-start(bf16[16,2,3072]{2,1,0:T(2,128)(2,1)} %reshape.180), calls=%async_computation.1 | async-start | bytes 393216 | tf_op jit(solution)/shard_map/all_to_all | solution.py:103
  57.7 0.2 select_reduce_fusion
  57.9 8.7 %all-to-all-done.1 = bf16[16,2,3072]{2,1,0:T(2,128)(2,1)S(1)} async-done(((bf16[16,2,3072]{2,1,0:T(2,128)(2,1)}), bf16[16,2,3072]{2,1,0:T(2,128)(2,1)S(1)}, u32[]{:S(2)}, u32[]{:S(2)}) %all-to-all-start.1) | async-done | bytes 196640 | tf_op jit(solution)/shard_map/all_to_all | solution.py:103
  66.6 0.1 reshape.181
  66.8 0.2 fusion.3
  67.0 0.6 add_convert_fusion
  (30 shorter events, 0.2 us)
Async XLA Ops:
  0.6 40.4 %copy-start = (bf16[1,1024,512]{2,1,0:T(8,128)(2,1)S(1)}, bf16[1,1024,512]{2,1,0:T(8,128)(2,1)}, u32[]{:S(2)}) copy-start(bf16[1,1024,512]{2,1,0:T(8,128)(2,1)} %param.29) | copy-start | bytes 3145732
  0.6 8.0 %copy-start.1 = (f32[16,2,128,128]{3,2,1,0:T(8,128)S(1)}, f32[16,2,128,128]{3,2,1,0:T(8,128)}, u32[]{:S(2)}) copy-start(f32[16,2,128,128]{3,2,1,0:T(8,128)} %param.17) | copy-start | bytes 6291460
  8.6 3.4 %copy-start.6 = (f32[2,128]{1,0:T(2,128)S(1)}, f32[2,128]{1,0:T(2,128)}, u32[]{:S(2)}) copy-start(f32[2,128]{1,0:T(2,128)} %param.22) | copy-start | bytes 3076
  8.6 10.1 %copy-start.3 = (bf16[16,1024]{1,0:T(8,128)(2,1)S(1)}, bf16[16,1024]{1,0:T(8,128)(2,1)}, u32[]{:S(2)}) copy-start(bf16[16,1024]{1,0:T(8,128)(2,1)} %param.16) | copy-start | bytes 98308
  8.7 10.3 %copy-start.5 = (f32[1024]{0:T(1024)S(1)}, f32[1024]{0:T(1024)}, u32[]{:S(2)}) copy-start(f32[1024]{0:T(1024)} %param.25) | copy-start | bytes 12292
  11.7 15.0 %copy-start.9 = (bf16[1024,4]{0,1:T(4,128)(2,1)S(1)}, bf16[1024,4]{0,1:T(4,128)(2,1)}, u32[]{:S(2)}) copy-start(bf16[1024,4]{0,1:T(4,128)(2,1)} %param.26) | copy-start | bytes 24580
  11.7 15.3 %copy-start.8 = (bf16[1024,16]{0,1:T(8,128)(2,1)S(1)}, bf16[1024,16]{0,1:T(8,128)(2,1)}, u32[]{:S(2)}) copy-start(bf16[1024,16]{0,1:T(8,128)(2,1)} %param.27) | copy-start | bytes 98308
  20.1 21.3 %copy-start.7 = (bf16[1,1024,512]{2,1,0:T(8,128)(2,1)S(1)}, bf16[1,1024,512]{2,1,0:T(8,128)(2,1)}, u32[]{:S(2)}) copy-start(bf16[1,1024,512]{2,1,0:T(8,128)(2,1)} %param.30) | copy-start | bytes 3145732
  20.1 20.8 %all-to-all-start = ((bf16[16,12,1024]{2,1,0:T(8,128)(2,1)}), bf16[16,12,1024]{2,1,0:T(8,128)(2,1)S(1)}, u32[]{:S(2)}, u32[]{:S(2)}) async-start(bf16[16,12,1024]{2,1,0:T(8,128)(2,1)} %reshape.168), calls=%async_computation | async-start | bytes 1048576 | tf_op jit(solution)/shard_map/all_to_all | solution.py:91
  41.4 8.0 %copy-start.2 = (bf16[1,1024,512]{2,1,0:T(8,128)(2,1)S(1)}, bf16[1,1024,512]{2,1,0:T(8,128)(2,1)}, u32[]{:S(2)}) copy-start(bf16[1,1024,512]{2,1,0:T(8,128)(2,1)} %param.31) | copy-start | bytes 3145732
  41.8 15.9 %copy-start.4 = (s32[16,6]{0,1:T(8,128)S(1)}, s32[16,6]{0,1:T(8,128)}, u32[]{:S(2)}) copy-start(s32[16,6]{0,1:T(8,128)} %param.28) | copy-start | bytes 1156
  53.3 13.4 %all-to-all-start.1 = ((bf16[16,2,3072]{2,1,0:T(2,128)(2,1)}), bf16[16,2,3072]{2,1,0:T(2,128)(2,1)S(1)}, u32[]{:S(2)}, u32[]{:S(2)}) async-start(bf16[16,2,3072]{2,1,0:T(2,128)(2,1)} %reshape.180), calls=%async_computation.1 | async-start | bytes 393216 | tf_op jit(solution)/shard_map/all_to_all | solution.py:103
